TPU v7x, 512 devices: a whole 4x4x16 slice. The times are simulated.
512 devices in a mesh: fs: 64 (over z, y), tp: 8 (over x, core).
Axes of the slice: x: 4, y: 4, z: 16, core: 2. Of those that a mesh axis runs over, the one named last changes fastest.
Arguments:
- saved_inputs: bfloat16 [49152, 2048], P('fs'), may hold values from -16 to 16
- input_cot: bfloat16 [49152, 2048], P('fs', 'tp'), may hold values from -0.02734375 to 0.02734375
- gate_cot: bfloat16 [49152, 2048], P('fs', 'tp'), may hold values from -0.02734375 to 0.02734375
- input_master: float32 [2048, 2048], P('fs', 'tp'), may hold values from -6 to 6
- gate_master: float32 [2048, 2048], P('fs', 'tp'), may hold values from -6 to 6
- input_factor: bfloat16 [2048, 256], P('fs'), may hold values from -2 to 2
- gate_factor: bfloat16 [2048, 256], P('fs'), may hold values from -2 to 2
- input_first: float32 [256, 2048], P('fs', 'tp'), may hold values from -6 to 6
- input_second: float32 [256, 2048], P('fs', 'tp'), may hold values from 0.2 to 17
- gate_first: float32 [256, 2048], P('fs', 'tp'), may hold values from -6 to 6
- gate_second: float32 [256, 2048], P('fs', 'tp'), may hold values from 0.2 to 17
Outputs:
- input_step: float32 [2048, 2048], P('fs', 'tp')
- gate_step: float32 [2048, 2048], P('fs', 'tp')
- input_first_new: float32 [256, 2048], P('fs', 'tp')
- input_second_new: float32 [256, 2048], P('fs', 'tp')
- gate_first_new: float32 [256, 2048], P('fs', 'tp')
- gate_second_new: float32 [256, 2048], P('fs', 'tp')
- input_copy: bfloat16 [2048, 2048], P(None, 'tp')
- gate_copy: bfloat16 [2048, 2048], P(None, 'tp')
All inputs are finite; a program needn't handle non-finite values.
Results may differ from a plain program's by a relative error of at most 0.0004.
Values may be sent and summed in bfloat16 or wider, within the bound.
A program may use at most 64 MiB of HBM per device.

v0:
```python
import jax
import jax.numpy as jnp
from jax import lax
from jax.sharding import Mesh
from jax.sharding import PartitionSpec as P

D = 2048
W = 2048
FS = ("fs_0", "fs_1")
FS_TP = ("fs_0", "fs_1", "tp_0", "tp_1")
TP = ("tp_0", "tp_1")
first_decay = 0.9
second_decay = 0.9
ratio_floor = 1e-08
mean_floor = 1e-06
step_size = 0.05


def own_block(parts, axes, order):
    shape = [lax.axis_size(a) for a in axes]
    parts = parts.reshape(*shape, *parts.shape[1:])
    parts = parts.transpose(*order, *range(len(axes), parts.ndim))
    parts = parts.reshape(-1, *parts.shape[len(axes) :])
    for k in order:
        parts = lax.psum_scatter(parts, axes[k], scatter_dimension=0, tiled=True)
    return parts[0]


def split_up(shard, dim, count):
    before, after = (shard.shape[:dim], shard.shape[dim + 1 :])
    return jnp.moveaxis(shard.reshape(*before, count, -1, *after), dim, 0)


def summed_rows(shard, axes, order, dim):
    count = lax.axis_size(axes)
    return own_block(split_up(shard, dim, count), axes, order)


def sent_and_summed(shard, axis, dim):
    count = lax.axis_size(axis)
    parts = lax.all_to_all(split_up(shard, dim, count), axis, 0, 0, tiled=True)
    return jnp.sum(parts, axis=0)


def sent_together(arrays, axis, dim, along):
    widths = [a.shape[along] for a in arrays]
    both = jnp.concatenate(arrays, axis=along)
    out = sent_and_summed(both, axis, dim)
    return tuple(jnp.split(out, [sum(widths[:k]) for k in range(1, len(widths))], axis=along))


def in_one_piece(arrays, axis, dim, along):
    both = jnp.concatenate(arrays, axis=along)
    out, at, finished = (lax.all_gather(both, axis, axis=dim, tiled=True), 0, [])
    for a in arrays:
        finished.append(lax.slice_in_dim(out, at, at + a.shape[along], axis=along))
        at += a.shape[along]
    return tuple(finished)


def one_axis_at_a_time(shard, axes):
    for axis in axes:
        shard = lax.psum(shard, axis)
    return shard


def moments(low_rank, first, second):
    first_new = first_decay * first + (1.0 - first_decay) * low_rank
    second_new = second_decay * second + (1.0 - second_decay) * low_rank * low_rank
    ratio = first_new / (jnp.sqrt(second_new) + ratio_floor)
    return (first_new, second_new, ratio)


def local(
    saved_inputs,
    input_cot,
    gate_cot,
    input_master,
    gate_master,
    input_factor,
    gate_factor,
    input_first,
    input_second,
    gate_first,
    gate_second,
):
    col_width = input_cot.shape[1]
    contract = (((0,), (0,)), ((), ()))
    factor_in = input_factor.astype(jnp.float32)
    factor_gate = gate_factor.astype(jnp.float32)
    term_in = lax.dot_general(saved_inputs, input_cot, contract, preferred_element_type=jnp.float32)
    term_gate = lax.dot_general(
        saved_inputs, gate_cot, contract, preferred_element_type=jnp.float32
    )
    gradients = summed_rows(jnp.concatenate([term_in, term_gate], axis=1), FS, (1, 0), 0)
    part_in = lax.dot_general(
        factor_in, gradients[:, :col_width], contract, precision=lax.Precision.HIGHEST
    )
    part_gate = lax.dot_general(
        factor_gate, gradients[:, col_width:], contract, precision=lax.Precision.HIGHEST
    )
    low_in, low_gate = sent_together((part_in, part_gate), FS, 0, 1)
    first_in, second_in, ratio_in = moments(low_in, input_first, input_second)
    first_gate, second_gate, ratio_gate = moments(low_gate, gate_first, gate_second)
    piece_in, piece_gate = in_one_piece((ratio_in, ratio_gate), FS, 0, 1)
    dir_in = jnp.dot(factor_in, piece_in, precision=lax.Precision.HIGHEST)
    dir_gate = jnp.dot(factor_gate, piece_gate, precision=lax.Precision.HIGHEST)
    square_in, square_gate = (
        one_axis_at_a_time(jnp.sum(dir_in * dir_in), FS_TP),
        one_axis_at_a_time(jnp.sum(dir_gate * dir_gate), FS_TP),
    )
    step_in = dir_in * lax.rsqrt(square_in / (D * W) + mean_floor)
    step_gate = dir_gate * lax.rsqrt(square_gate / (D * W) + mean_floor)
    local_in = (input_master - step_size * step_in).astype(jnp.bfloat16)
    local_gate = (gate_master - step_size * step_gate).astype(jnp.bfloat16)
    copy_in, copy_gate = in_one_piece((local_in, local_gate), FS, 0, 1)
    return (step_in, step_gate, first_in, second_in, first_gate, second_gate, copy_in, copy_gate)


def solution(mesh):
    finer = Mesh(mesh.devices.reshape(16, 4, 4, 2), ("fs_0", "fs_1", "tp_0", "tp_1"))
    placed = (
        P(FS, None),
        P(FS, TP),
        P(FS, TP),
        P(FS, TP),
        P(FS, TP),
        P(FS, None),
        P(FS, None),
        P(FS, TP),
        P(FS, TP),
        P(FS, TP),
        P(FS, TP),
    )
    return jax.shard_map(
        local,
        mesh=finer,
        in_specs=placed,
        out_specs=(
            P(FS, TP),
            P(FS, TP),
            P(FS, TP),
            P(FS, TP),
            P(FS, TP),
            P(FS, TP),
            P(None, TP),
            P(None, TP),
        ),
        check_vma=False,
    )
```

profile of v0, /device:TPU:2, one launch (start us, length us, event | category | flops | bytes accessed | tf_op | source)
XLA Modules:
  0.0 511.1 jit_solution(1282623223704920424)
XLA Ops:
  7.2 1.8 copy-done
  9.1 2.0 fusion.11
  11.1 1.0 fusion.12
  12.1 2.5 pad_maximum_fusion
  14.6 5.3 %copy.22 = f32[2048,512]{1,0:T(8,128)} copy(f32[2048,512]{0,1:T(8,128)} %pad_maximum_fusion) | data formatting | bytes 8388608 | tf_op jit(solution)/shard_map/concatenate | solution.py:95
  19.9 5.0 copy.23
  25.0 59.1 %reduce-scatter.3.cloned.1.call-done = f32[16,32,512]{2,1,0:T(8,128)} async-done(((f32[64,32,512]{2,1,0:T(8,128)}), f32[16,32,512]{2,1,0:T(8,128)}) %reduce-scatter.3.cloned.1.call-update) | async-done | bytes 1048592 | tf_op jit(solution)/shard_map/reduce_scatter | solution.py:25
  84.1 73.8 %reduce-scatter.5.cloned.1.call-done = f32[1,32,512]{2,1,0:T(8,128)} async-done(((f32[16,32,512]{2,1,0:T(8,128)}), f32[1,32,512]{2,1,0:T(8,128)}) %reduce-scatter.5.cloned.1.call-update) | async-done | bytes 65552 | tf_op jit(solution)/shard_map/reduce_scatter | solution.py:25
  158.0 1.1 convolution_bitcast_fusion
  159.1 1.1 convolution_bitcast_fusion.1
  161.0 2.0 copy.24
  163.0 2.0 reshape.23
  165.0 35.0 %all_to_all.5 = f32[64,4,512]{2,1,0:T(4,128)} all-to-all(f32[64,4,512]{2,1,0:T(4,128)} %reshape.23), channel_id=1, replica_groups=mesh['fs_0'=16,'fs_1'=4,'tp_0'=4,'tp_1'=2] {'fs_0','fs_1'}, dimensions={0} | all-to-all | bytes 1048576 | tf_op jit(solution)/shard_map/all_to_all | solution.py:41
  200.0 1.2 reduce_sum.27
  201.8 107.3 %all-gather = f32[64,4,512]{2,1,0:T(4,128)} all-gather(f32[1,4,512]{2,1,0:T(4,128)S(1)} %maximum_bitcast_fusion), channel_id=1, replica_groups=mesh['fs_0'=16,'fs_1'=4,'tp_0'=4,'tp_1'=2] {'fs_0','fs_1'}, dimensions={0}, use_global_device_ids=true | all-gather | bytes 532480 | tf_op jit(solution)/shard_map/all_gather | solution.py:54
  309.1 2.0 reshape.25
  311.1 1.8 multiply_reduce_fusion
  312.9 1.8 multiply_reduce_fusion.1
  314.7 28.8 %all-reduce = (f32[]{:T(128)}, f32[]{:T(128)}) all-reduce(f32[]{:T(128)} %get-tuple-element.31, f32[]{:T(128)} %get-tuple-element.33), channel_id=1, replica_groups=mesh['fs_0'=16,'fs_1'=4,'tp_0'=4,'tp_1'=2] {'fs_0'}, use_global_device_ids=true, to_apply=%region_4.0 | all-reduce | flops 2 | bytes 16 | tf_op jit(solution)/shard_map/psum | solution.py:63
  343.5 10.7 %all-reduce.2 = (f32[]{:T(128)}, f32[]{:T(128)}) all-reduce(f32[]{:T(128)} %get-tuple-element.8, f32[]{:T(128)} %get-tuple-element.9), channel_id=1, replica_groups=mesh['fs_0'=16,'fs_1'=4,'tp_0'=4,'tp_1'=2] {'fs_1'}, use_global_device_ids=true, to_apply=%region_5.0 | all-reduce | flops 2 | bytes 16 | tf_op jit(solution)/shard_map/psum | solution.py:63
  354.2 9.3 %all-reduce.1 = (f32[]{:T(128)}, f32[]{:T(128)}) all-reduce(f32[]{:T(128)} %get-tuple-element.12, f32[]{:T(128)} %get-tuple-element.13), channel_id=1, replica_groups=mesh['fs_0'=16,'fs_1'=4,'tp_0'=4,'tp_1'=2] {'tp_0'}, use_global_device_ids=true, to_apply=%region_6.0 | all-reduce | flops 2 | bytes 16 | tf_op jit(solution)/shard_map/psum | solution.py:63
  363.5 3.1 all-reduce.3
  369.3 132.4 %all-gather.3.cloned.1.call-done = bf16[2048,512]{1,0:T(8,128)(2,1)} async-done(((bf16[32,512]{1,0:T(8,128)(2,1)}), bf16[2048,512]{1,0:T(8,128)(2,1)}) %all-gather.3.cloned.1.call-update) | async-done | bytes 2097168 | tf_op jit(solution)/shard_map/all_gather | solution.py:54
  501.6 3.0 fusion.10
  (30 shorter events, 2.9 us)
Async XLA Ops:
  7.2 1.9 copy-start
  7.2 3.9 copy-start.1
  7.2 76.9 %reduce-scatter.3.cloned.1.call-start = ((), (), s32[]{:S(2)}) async-start(), calls=%async_computation.3 | async-start | bytes 5242880 | tf_op jit(solution)/shard_map/reduce_scatter | solution.py:25
  24.9 133.1 %copy-start.2 = (bf16[32,256]{1,0:T(8,128)(2,1)S(1)}, bf16[32,256]{1,0:T(8,128)(2,1)}, u32[]{:S(2)}) copy-start(bf16[32,256]{1,0:T(8,128)(2,1)} %param.17) | copy-start | bytes 49156
  24.9 134.2 %copy-start.3 = (bf16[32,256]{1,0:T(8,128)(2,1)S(1)}, bf16[32,256]{1,0:T(8,128)(2,1)}, u32[]{:S(2)}) copy-start(bf16[32,256]{1,0:T(8,128)(2,1)} %param.16) | copy-start | bytes 49156
  24.9 133.0 %reduce-scatter.5.cloned.1.call-start = ((), (), s32[]{:S(2)}) async-start(), calls=%async_computation.4 | async-start | bytes 1114112 | tf_op jit(solution)/shard_map/reduce_scatter | solution.py:25
  84.1 117.1 %copy-start.6 = (f32[4,256]{1,0:T(4,128)S(1)}, f32[4,256]{1,0:T(4,128)}, u32[]{:S(2)}) copy-start(f32[4,256]{1,0:T(4,128)} %param.19) | copy-start | bytes 12292
  84.1 117.1 %copy-start.7 = (f32[4,256]{1,0:T(4,128)S(1)}, f32[4,256]{1,0:T(4,128)}, u32[]{:S(2)}) copy-start(f32[4,256]{1,0:T(4,128)} %param.18) | copy-start | bytes 12292
  84.1 117.1 %copy-start.8 = (f32[4,256]{1,0:T(4,128)S(1)}, f32[4,256]{1,0:T(4,128)}, u32[]{:S(2)}) copy-start(f32[4,256]{1,0:T(4,128)} %param.21) | copy-start | bytes 12292
  84.1 117.1 %copy-start.9 = (f32[4,256]{1,0:T(4,128)S(1)}, f32[4,256]{1,0:T(4,128)}, u32[]{:S(2)}) copy-start(f32[4,256]{1,0:T(4,128)} %param.20) | copy-start | bytes 12292
  84.1 417.5 %all-gather.3.cloned.1.call-start = ((), (), s32[]{:S(2)}) async-start(), calls=%async_computation.5 | async-start | bytes 2129920 | tf_op jit(solution)/shard_map/all_gather | solution.py:54
  161.0 207.0 %copy-start.4 = (f32[32,256]{1,0:T(8,128)S(1)}, f32[32,256]{1,0:T(8,128)}, u32[]{:S(2)}) copy-start(f32[32,256]{1,0:T(8,128)} %param.15) | copy-start | bytes 98308
  161.0 207.0 %copy-start.5 = (f32[32,256]{1,0:T(8,128)S(1)}, f32[32,256]{1,0:T(8,128)}, u32[]{:S(2)}) copy-start(f32[32,256]{1,0:T(8,128)} %param.14) | copy-start | bytes 98308
Sparse Core Ops, SparseCore 0:
  25.0 58.9 reduce-scatter.2
  86.9 71.0 reduce-scatter.4
  369.4 132.1 all-gather.2
where the time goes:
time: 512 us; the launch traced here: 511 us
  waiting for transfers between devices  265 us (52%)
  blocking collectives  194 us (38%)
  local copies, waits for them, and re-layouts  21.2 us (4%)
  between operations  15.2 us (3%)
  matrix products  8.73 us (2%)
  other arithmetic  6.31 us (1%)
    reduce_scatter x2, waiting for transfers between devices, own_block(): parts = lax.psum_scatter(parts, axes[k], scatter_dimension=0, tiled=True)  133 us
    all_gather x1, waiting for transfers between devices, in_one_piece(): lax.all_gather(both, axis, axis=dim, tiled=True)  132 us
    all_gather x1, blocking collectives, in_one_piece(): lax.all_gather(both, axis, axis=dim, tiled=True)  107 us
    psum x4, blocking collectives, one_axis_at_a_time(): shard = lax.psum(shard, axis)  51.9 us
    all_to_all x1, blocking collectives, sent_and_summed(): parts = lax.all_to_all(split_up(shard, dim, count), axis, 0, 0, tiled=True)  35 us
  transfers between devices with their start and end apart: 3, of which 3 were waited for; matrix products, arithmetic and copies ran while one was open for 0% of the time, Pallas kernels for 0%

commit v1 on v0

--- a/solution.py
+++ b/solution.py
@@ -60,7 +60,8 @@
 
 def one_axis_at_a_time(shard, axes):
     for axis in axes:
-        shard = lax.psum(shard, axis)
+        pieces = lax.all_gather(shard, axis, axis=0, tiled=False)
+        shard = pieces.sum(axis=0)
     return shard
 
 

time: 512 us -> 528 us (1.031)
  blocking collectives: 194 us -> 157 us
  waiting for transfers between devices: 265 us -> 285 us
  local copies, waits for them, and re-layouts: 21.2 us -> 37.7 us
  starting transfers between devices: 0.12 us -> 12.3 us
    psum x4 -> x0, blocking collectives: 51.9 us -> none  [one_axis_at_a_time(): shard = lax.psum(shard, axis)]
    unnamed x0 -> x4, blocking collectives: none -> 48.9 us
    all_to_all x1 -> x0, blocking collectives: 35 us -> none  [sent_and_summed(): parts = lax.all_to_all(split_up(shard, dim, count), axis, 0, 0, tiled=True)]
    all_to_all x0 -> x1, waiting for transfers between devices: none -> 20.2 us  [sent_and_summed(): parts = lax.all_to_all(split_up(shard, dim, count), axis, 0, 0, tiled=True)]
    unnamed x21 -> x41, local copies, waits for them, and re-layouts: 3.88 us -> 20.3 us
    all_to_all x0 -> x1, starting transfers between devices: none -> 12.2 us  [sent_and_summed(): parts = lax.all_to_all(split_up(shard, dim, count), axis, 0, 0, tiled=True)]
  transfers between devices with their start and end apart: 3 -> 4, of which waited for: 3 -> 4; matrix products, arithmetic and copies ran while one was open for 0% -> 0% of each run, Pallas kernels for 0% -> 0%
where the time goes in v1:
time: 528 us; the launch traced here: 527 us
  waiting for transfers between devices  285 us (54%)
  blocking collectives  157 us (30%)
  local copies, waits for them, and re-layouts  37.7 us (7%)
  between operations  15.3 us (3%)
  starting transfers between devices  12.3 us (2%)
  other arithmetic  11.1 us (2%)
  matrix products  8.74 us (2%)
    reduce_scatter x2, waiting for transfers between devices, own_block(): parts = lax.psum_scatter(parts, axes[k], scatter_dimension=0, tiled=True)  133 us
    all_gather x1, waiting for transfers between devices, in_one_piece(): lax.all_gather(both, axis, axis=dim, tiled=True)  132 us
    all_gather x1, blocking collectives, in_one_piece(): lax.all_gather(both, axis, axis=dim, tiled=True)  108 us
    unnamed x4, blocking collectives  48.9 us
    unnamed x41, local copies, waits for them, and re-layouts  20.3 us
    all_to_all x1, waiting for transfers between devices, sent_and_summed(): parts = lax.all_to_all(split_up(shard, dim, count), axis, 0, 0, tiled=True)  20.2 us
    all_to_all x1, starting transfers between devices, sent_and_summed(): parts = lax.all_to_all(split_up(shard, dim, count), axis, 0, 0, tiled=True)  12.2 us
  transfers between devices with their start and end apart: 4, of which 4 were waited for; matrix products, arithmetic and copies ran while one was open for 0% of the time, Pallas kernels for 0%

profile of v1, /device:TPU:2, one launch (start us, length us, event | category | flops | bytes accessed | tf_op | source)
XLA Modules:
  0.0 527.1 jit_solution(2903521578319546647)
XLA Ops:
  7.2 1.8 copy-done
  9.1 2.0 fusion.11
  12.1 2.5 pad_maximum_fusion
  14.6 5.3 %copy.22 = f32[2048,512]{1,0:T(8,128)} copy(f32[2048,512]{0,1:T(8,128)} %pad_maximum_fusion) | data formatting | bytes 8388608 | tf_op jit(solution)/shard_map/concatenate | solution.py:96
  19.9 5.0 copy.23
  25.0 59.1 %reduce-scatter.3.cloned.1.call-done = f32[16,32,512]{2,1,0:T(8,128)} async-done(((f32[64,32,512]{2,1,0:T(8,128)}), f32[16,32,512]{2,1,0:T(8,128)}) %reduce-scatter.3.cloned.1.call-update) | async-done | bytes 1048592 | tf_op jit(solution)/shard_map/reduce_scatter | solution.py:25
  84.1 73.9 %reduce-scatter.5.cloned.1.call-done = f32[1,32,512]{2,1,0:T(8,128)} async-done(((f32[16,32,512]{2,1,0:T(8,128)}), f32[1,32,512]{2,1,0:T(8,128)}) %reduce-scatter.5.cloned.1.call-update) | async-done | bytes 65552 | tf_op jit(solution)/shard_map/reduce_scatter | solution.py:25
  161.0 2.0 copy.24
  163.0 2.0 reshape.23
  165.0 12.2 %all-to-all-start = ((f32[64,4,512]{2,1,0:T(4,128)}), f32[64,4,512]{2,1,0:T(4,128)}, u32[]{:S(2)}, u32[]{:S(2)}) async-start(f32[64,4,512]{2,1,0:T(4,128)} %reshape.23), calls=%async_computation.2 | async-start | bytes 1048576 | tf_op jit(solution)/shard_map/all_to_all | solution.py:41
  179.9 20.2 %all-to-all-done = f32[64,4,512]{2,1,0:T(4,128)} async-done(((f32[64,4,512]{2,1,0:T(4,128)}), f32[64,4,512]{2,1,0:T(4,128)}, u32[]{:S(2)}, u32[]{:S(2)}) %all-to-all-start) | async-done | bytes 524320 | tf_op jit(solution)/shard_map/all_to_all | solution.py:41
  201.9 107.9 %all-gather = f32[64,4,512]{2,1,0:T(4,128)} all-gather(f32[1,4,512]{2,1,0:T(4,128)S(1)} %maximum_bitcast_fusion), channel_id=1, replica_groups=mesh['fs_0'=16,'fs_1'=4,'tp_0'=4,'tp_1'=2] {'fs_0','fs_1'}, dimensions={0}, use_global_device_ids=true | all-gather | bytes 532480 | tf_op jit(solution)/shard_map/all_gather | solution.py:54
  309.8 2.0 reshape.49
  311.8 1.8 multiply_reduce_fusion.1
  313.6 1.8 multiply_reduce_fusion
  316.8 1.4 dynamic-update-slice.4
  318.2 27.5 %all-reduce.8 = (f32[16]{0:T(128)S(1)}, f32[16]{0:T(128)S(1)}) all-reduce(f32[16]{0:T(128)S(1)} %dynamic-update-slice, f32[16]{0:T(128)S(1)} %dynamic-update-slice.4), channel_id=1, replica_groups=mesh['fs_0'=16,'fs_1'=4,'tp_0'=4,'tp_1'=2] {'fs_0'}, use_global_device_ids=true, to_apply=%add | all-reduce | flops 32 | bytes 256
  346.9 1.4 dynamic-update-slice.5
  348.3 1.4 dynamic-update-slice.1
  351.0 10.3 %all-reduce.10 = (f32[4]{0:T(128)S(1)}, f32[4]{0:T(128)S(1)}) all-reduce(f32[4]{0:T(128)S(1)} %dynamic-update-slice.1, f32[4]{0:T(128)S(1)} %dynamic-update-slice.5), channel_id=1, replica_groups=mesh['fs_0'=16,'fs_1'=4,'tp_0'=4,'tp_1'=2] {'fs_1'}, use_global_device_ids=true, to_apply=%add.1 | all-reduce | flops 8 | bytes 64
  366.6 8.6 %all-reduce.9 = (f32[4]{0:T(128)S(1)}, f32[4]{0:T(128)S(1)}) all-reduce(f32[4]{0:T(128)S(1)} %dynamic-update-slice.2, f32[4]{0:T(128)S(1)} %dynamic-update-slice.6), channel_id=1, replica_groups=mesh['fs_0'=16,'fs_1'=4,'tp_0'=4,'tp_1'=2] {'tp_0'}, use_global_device_ids=true, to_apply=%add.2 | all-reduce | flops 8 | bytes 64
  379.3 2.4 all-reduce.11
  385.6 132.0 %all-gather.3.cloned.1.call-done = bf16[2048,512]{1,0:T(8,128)(2,1)} async-done(((bf16[32,512]{1,0:T(8,128)(2,1)}), bf16[2048,512]{1,0:T(8,128)(2,1)}) %all-gather.3.cloned.1.call-update) | async-done | bytes 2097168 | tf_op jit(solution)/shard_map/all_gather | solution.py:54
  517.6 3.0 fusion.10
  (59 shorter events, 24.2 us)
Async XLA Ops:
  7.2 1.9 copy-start
  7.2 3.9 copy-start.1
  7.2 76.9 %reduce-scatter.3.cloned.1.call-start = ((), (), s32[]{:S(2)}) async-start(), calls=%async_computation.3 | async-start | bytes 5242880 | tf_op jit(solution)/shard_map/reduce_scatter | solution.py:25
  24.9 133.1 %copy-start.3 = (bf16[32,256]{1,0:T(8,128)(2,1)S(1)}, bf16[32,256]{1,0:T(8,128)(2,1)}, u32[]{:S(2)}) copy-start(bf16[32,256]{1,0:T(8,128)(2,1)} %param.17) | copy-start | bytes 49156
  24.9 134.2 %copy-start.2 = (bf16[32,256]{1,0:T(8,128)(2,1)S(1)}, bf16[32,256]{1,0:T(8,128)(2,1)}, u32[]{:S(2)}) copy-start(bf16[32,256]{1,0:T(8,128)(2,1)} %param.16) | copy-start | bytes 49156
  24.9 133.0 %reduce-scatter.5.cloned.1.call-start = ((), (), s32[]{:S(2)}) async-start(), calls=%async_computation.4 | async-start | bytes 1114112 | tf_op jit(solution)/shard_map/reduce_scatter | solution.py:25
  84.1 117.1 %copy-start.6 = (f32[4,256]{1,0:T(4,128)S(1)}, f32[4,256]{1,0:T(4,128)}, u32[]{:S(2)}) copy-start(f32[4,256]{1,0:T(4,128)} %param.19) | copy-start | bytes 12292
  84.1 117.1 %copy-start.7 = (f32[4,256]{1,0:T(4,128)S(1)}, f32[4,256]{1,0:T(4,128)}, u32[]{:S(2)}) copy-start(f32[4,256]{1,0:T(4,128)} %param.18) | copy-start | bytes 12292
  84.1 117.2 %copy-start.8 = (f32[4,256]{1,0:T(4,128)S(1)}, f32[4,256]{1,0:T(4,128)}, u32[]{:S(2)}) copy-start(f32[4,256]{1,0:T(4,128)} %param.21) | copy-start | bytes 12292
  84.1 117.2 %copy-start.9 = (f32[4,256]{1,0:T(4,128)S(1)}, f32[4,256]{1,0:T(4,128)}, u32[]{:S(2)}) copy-start(f32[4,256]{1,0:T(4,128)} %param.20) | copy-start | bytes 12292
  161.0 223.3 %copy-start.4 = (f32[32,256]{1,0:T(8,128)S(1)}, f32[32,256]{1,0:T(8,128)}, u32[]{:S(2)}) copy-start(f32[32,256]{1,0:T(8,128)} %param.15) | copy-start | bytes 98308
  161.0 223.3 %copy-start.5 = (f32[32,256]{1,0:T(8,128)S(1)}, f32[32,256]{1,0:T(8,128)}, u32[]{:S(2)}) copy-start(f32[32,256]{1,0:T(8,128)} %param.14) | copy-start | bytes 98308
  165.0 35.1 %all-to-all-start = ((f32[64,4,512]{2,1,0:T(4,128)}), f32[64,4,512]{2,1,0:T(4,128)}, u32[]{:S(2)}, u32[]{:S(2)}) async-start(f32[64,4,512]{2,1,0:T(4,128)} %reshape.23), calls=%async_computation.2 | async-start | bytes 1048576 | tf_op jit(solution)/shard_map/all_to_all | solution.py:41
  177.2 340.4 %all-gather.3.cloned.1.call-start = ((), (), s32[]{:S(2)}) async-start(), calls=%async_computation.5 | async-start | bytes 2129920 | tf_op jit(solution)/shard_map/all_gather | solution.py:54
Sparse Core Ops, SparseCore 0:
  25.1 58.9 reduce-scatter.2
  86.9 71.0 reduce-scatter.4
  385.7 131.8 all-gather.2
